TPU v7x, 32 devices: a whole 2x2x4 slice. The times are simulated.
32 devices in a mesh: ra: 4 (over y, x), cb: 8 (over z, core).
Axes of the slice: x: 2, y: 2, z: 4, core: 2. Of those that a mesh axis runs over, the one named last changes fastest.
Arguments:
- tokens: bfloat16 [512, 4096], P(None, 'ra'), may hold values from -40 to 40, as said below
- norm_gain: float32 [2, 4096], P(None, 'ra'), may hold values from 0.1 to 1.9
- gate_weight: bfloat16 [2, 4096, 11264], P(None, 'ra', 'cb'), may hold values from -0.09375 to 0.09375
- up_weight: bfloat16 [2, 4096, 11264], P(None, 'ra', 'cb'), may hold values from -0.09375 to 0.09375
- down_weight: bfloat16 [2, 11264, 4096], P(None, 'cb', 'ra'), may hold values from -0.0546875 to 0.0546875
Outputs:
- result: bfloat16 [512, 4096], P(None, 'ra')
Inputs may be any that keep to these rules, and one draw needn't show every extreme that they name: `tokens`: features come in blocks of 32 with scales that differ from block to block by up to a factor of 16.
All inputs are finite; a program needn't handle non-finite values.
Results may differ from a plain program's by a relative error of at most 0.0075.
Values may be sent and summed in bfloat16 or wider, within the bound.
A program may use at most 64 MiB of HBM per device.

v0:
```python
import jax
import jax.numpy as jnp
from jax import lax
from jax.sharding import PartitionSpec as P

D = 4096
LAYERS = 2
epsilon = 1e-06
keep_share = 0.5


def body(tokens, norm_gain, gate_weight, up_weight, down_weight):
    stream = tokens
    for layer in range(LAYERS):
        widened = stream.astype(jnp.float32)
        squares = jnp.sum(widened * widened, axis=1)
        normed = (widened * norm_gain[layer]).astype(jnp.bfloat16)
        gate_part = jnp.dot(normed, gate_weight[layer], preferred_element_type=jnp.float32)
        up_part = jnp.dot(normed, up_weight[layer], preferred_element_type=jnp.float32)
        total = lax.psum(squares, "ra")
        gate_share, up_share = (
            lax.psum_scatter(gate_part, "ra", scatter_dimension=1, tiled=True),
            lax.psum_scatter(up_part, "ra", scatter_dimension=1, tiled=True),
        )
        scale = lax.rsqrt(total / D + epsilon)[:, None]
        share = (jax.nn.silu(gate_share * scale) * (up_share * scale)).astype(jnp.bfloat16)
        hidden = lax.all_gather(share, "ra", axis=1, tiled=True)
        partial_down = jnp.dot(hidden, down_weight[layer], preferred_element_type=jnp.float32)
        branch = lax.psum(partial_down, "cb")
        stream = (keep_share * widened + branch).astype(jnp.bfloat16)
    return stream


def solution(mesh):
    placed = (
        P(None, "ra"),
        P(None, "ra"),
        P(None, "ra", "cb"),
        P(None, "ra", "cb"),
        P(None, "cb", "ra"),
    )
    return jax.shard_map(body, mesh=mesh, in_specs=placed, out_specs=P(None, "ra"), check_vma=False)
```

profile of v0, /device:TPU:0, one launch (start us, length us, event | category | flops | bytes accessed | tf_op | source)
XLA Modules:
  0.0 411.4 jit_solution(7383496427016766130)
XLA Ops:
  6.5 0.8 fusion.31
  7.3 5.4 %fusion.8 = f32[512,1408]{0,1:T(8,128)} fusion(bf16[2,1024,1408]{2,1,0:T(8,128)(2,1)} %param.8, bf16[512,1024]{1,0:T(8,128)(2,1)} %param.5, f32[1024]{0:T(1024)S(1)} %bitcast.24), kind=kOutput, calls=%fused_computation.14 | convolution fusion | flops 1477967872 | bytes 6819840 | tf_op jit(solution)/shard_map/dot_general | solution.py:19
  12.7 0.0 reduce-scatter.7.cloned.1.call-update
  12.8 0.0 reduce-scatter.5.cloned.1.call-start
  12.8 1.1 copy-done
  14.0 5.1 %fusion.10 = f32[512,1408]{0,1:T(8,128)} fusion(bf16[2,1024,1408]{2,1,0:T(8,128)(2,1)} %param.7, bf16[512,1024]{1,0:T(8,128)(2,1)S(1)} %copy-done, f32[1024]{0:T(1024)S(1)} %bitcast.25), kind=kOutput, calls=%fused_computation.16 | convolution fusion | flops 1477967872 | bytes 6819840 | tf_op jit(solution)/shard_map/dot_general | solution.py:18
  19.1 0.0 reduce-scatter.5.cloned.1.call-update
  19.1 0.0 all-gather.3.cloned.1.call-start
  19.2 0.3 fusion.21
  19.5 11.9 %psum.28 = f32[512]{0:T(512)S(1)} all-reduce(f32[512]{0:T(512)S(1)} %fusion.21), channel_id=1, replica_groups=mesh['ra'=4,'cb'=8] {'ra'}, use_global_device_ids=true, to_apply=%region_2.0 | all-reduce | flops 512 | bytes 4096 | tf_op jit(solution)/shard_map/psum | solution.py:20
  31.4 26.3 %reduce-scatter.7.cloned.1.call-done = f32[512,352]{0,1:T(8,128)} async-done(((f32[512,1408]{0,1:T(8,128)}), f32[512,352]{0,1:T(8,128)}) %reduce-scatter.7.cloned.1.call-update) | async-done | bytes 720912 | tf_op jit(solution)/shard_map/reduce_scatter | solution.py:23
  57.6 44.8 %reduce-scatter.5.cloned.1.call-done = f32[512,352]{0,1:T(8,128)} async-done(((f32[512,1408]{0,1:T(8,128)}), f32[512,352]{0,1:T(8,128)}) %reduce-scatter.5.cloned.1.call-update) | async-done | bytes 720912 | tf_op jit(solution)/shard_map/reduce_scatter | solution.py:22
  102.4 2.3 multiply_convert_fusion.1
  104.7 0.0 all-reduce.3.cloned.1.call-start
  104.8 29.8 %all-gather.3.cloned.1.call-done = bf16[512,1408]{0,1:T(8,128)(2,1)} async-done(((bf16[512,352]{0,1:T(8,128)(2,1)}), bf16[512,1408]{0,1:T(8,128)(2,1)}) %all-gather.3.cloned.1.call-update) | async-done | bytes 1441808 | tf_op jit(solution)/shard_map/all_gather | solution.py:27
  134.6 5.4 %fusion.6 = f32[512,1024]{1,0:T(8,128)} fusion(bf16[512,1408]{0,1:T(8,128)(2,1)} %all-gather.3.cloned.1.call-done, bf16[2,1408,1024]{2,1,0:T(8,128)(2,1)} %param.9), kind=kOutput, calls=%fused_computation.12 | convolution fusion | flops 1476395008 | bytes 6422528 | tf_op jit(solution)/shard_map/dot_general | solution.py:28
  140.1 0.0 reduce-scatter.9.cloned.1.call-start
  140.1 65.2 %all-reduce.3.cloned.1.call-done = f32[512,1024]{1,0:T(8,128)} async-done(((f32[512,1024]{1,0:T(8,128)}), f32[512,1024]{1,0:T(8,128)}) %all-reduce.3.cloned.1.call-update) | async-done | bytes 2097168 | tf_op jit(solution)/shard_map/psum | solution.py:29
  205.3 2.0 fusion.25
  207.4 5.1 %fusion.4 = f32[512,1408]{0,1:T(8,128)} fusion(bf16[2,1024,1408]{2,1,0:T(8,128)(2,1)} %param.7, bf16[512,1024]{1,0:T(8,128)(2,1)S(1)} %get-tuple-element.6, f32[1024]{0:T(1024)S(1)} %bitcast.22), kind=kOutput, calls=%fused_computation.10 | convolution fusion | flops 1477967872 | bytes 6819840 | tf_op jit(solution)/shard_map/dot_general | solution.py:18
  212.5 0.0 reduce-scatter.11.cloned.1.call-start
  212.5 5.1 %fusion.2 = f32[512,1408]{0,1:T(8,128)} fusion(bf16[2,1024,1408]{2,1,0:T(8,128)(2,1)} %param.8, bf16[512,1024]{1,0:T(8,128)(2,1)S(1)} %get-tuple-element.6, f32[1024]{0:T(1024)S(1)} %bitcast.23), kind=kOutput, calls=%fused_computation.8 | convolution fusion | flops 1477967872 | bytes 6819840 | tf_op jit(solution)/shard_map/dot_general | solution.py:19
  217.7 0.0 all-gather.5.cloned.1.call-start
  217.7 10.4 %psum.30 = f32[512]{0:T(512)S(1)} all-reduce(f32[512]{0:T(512)S(1)} %get-tuple-element.5), channel_id=1, replica_groups=mesh['ra'=4,'cb'=8] {'ra'}, use_global_device_ids=true, to_apply=%region_7.8 | all-reduce | flops 512 | bytes 4096 | tf_op jit(solution)/shard_map/psum | solution.py:20
  228.1 26.0 %reduce-scatter.9.cloned.1.call-done = f32[512,352]{0,1:T(8,128)} async-done(((f32[512,1408]{0,1:T(8,128)}), f32[512,352]{0,1:T(8,128)}) %reduce-scatter.9.cloned.1.call-update) | async-done | bytes 720912 | tf_op jit(solution)/shard_map/reduce_scatter | solution.py:22
  254.1 44.7 %reduce-scatter.11.cloned.1.call-done = f32[512,352]{0,1:T(8,128)} async-done(((f32[512,1408]{0,1:T(8,128)}), f32[512,352]{0,1:T(8,128)}) %reduce-scatter.11.cloned.1.call-update) | async-done | bytes 720912 | tf_op jit(solution)/shard_map/reduce_scatter | solution.py:23
  298.8 2.3 multiply_convert_fusion
  301.1 0.0 all-reduce.5.cloned.1.call-start
  301.1 29.9 %all-gather.5.cloned.1.call-done = bf16[512,1408]{0,1:T(8,128)(2,1)} async-done(((bf16[512,352]{0,1:T(8,128)(2,1)}), bf16[512,1408]{0,1:T(8,128)(2,1)}) %all-gather.5.cloned.1.call-update) | async-done | bytes 1441808 | tf_op jit(solution)/shard_map/all_gather | solution.py:27
  331.0 5.4 %fusion = f32[512,1024]{1,0:T(8,128)} fusion(bf16[512,1408]{0,1:T(8,128)(2,1)} %all-gather.5.cloned.1.call-done, bf16[2,1408,1024]{2,1,0:T(8,128)(2,1)} %param.9), kind=kOutput, calls=%fused_computation.6 | convolution fusion | flops 1476395008 | bytes 6422528 | tf_op jit(solution)/shard_map/dot_general | solution.py:28
  336.5 65.2 %all-reduce.5.cloned.1.call-done = f32[512,1024]{1,0:T(8,128)} async-done(((f32[512,1024]{1,0:T(8,128)}), f32[512,1024]{1,0:T(8,128)}) %all-reduce.5.cloned.1.call-update) | async-done | bytes 2097168 | tf_op jit(solution)/shard_map/psum | solution.py:29
  401.7 2.9 fusion.23
  (10 shorter events, 0.1 us)
Async XLA Ops:
  6.5 51.1 %reduce-scatter.7.cloned.1.call-start = ((), (), s32[]{:S(2)}) async-start(), calls=%async_computation.5 | async-start | bytes 3604480 | tf_op jit(solution)/shard_map/reduce_scatter | solution.py:23
  12.7 1.2 copy-start
  12.8 89.7 %reduce-scatter.5.cloned.1.call-start = ((), (), s32[]{:S(2)}) async-start(), calls=%async_computation.4 | async-start | bytes 3604480 | tf_op jit(solution)/shard_map/reduce_scatter | solution.py:22
  19.1 115.5 %all-gather.3.cloned.1.call-start = ((), (), s32[]{:S(2)}) async-start(), calls=%async_computation.6 | async-start | bytes 1802240 | tf_op jit(solution)/shard_map/all_gather | solution.py:27
  104.7 100.6 %all-reduce.3.cloned.1.call-start = ((), (), s32[]{:S(2)}) async-start(), calls=%async_computation.7 | async-start | bytes 4194304 | tf_op jit(solution)/shard_map/psum | solution.py:29
  140.1 114.1 %reduce-scatter.9.cloned.1.call-start = ((), (), s32[]{:S(2)}) async-start(), calls=%async_computation.8 | async-start | bytes 3604480 | tf_op jit(solution)/shard_map/reduce_scatter | solution.py:22
  212.5 86.3 %reduce-scatter.11.cloned.1.call-start = ((), (), s32[]{:S(2)}) async-start(), calls=%async_computation.9 | async-start | bytes 3604480 | tf_op jit(solution)/shard_map/reduce_scatter | solution.py:23
  217.7 113.3 %all-gather.5.cloned.1.call-start = ((), (), s32[]{:S(2)}) async-start(), calls=%async_computation.10 | async-start | bytes 1802240 | tf_op jit(solution)/shard_map/all_gather | solution.py:27
  301.1 100.6 %all-reduce.5.cloned.1.call-start = ((), (), s32[]{:S(2)}) async-start(), calls=%async_computation.11 | async-start | bytes 4194304 | tf_op jit(solution)/shard_map/psum | solution.py:29
Sparse Core Ops, SparseCore 0:
  12.9 44.7 reduce-scatter.6
  60.7 41.7 reduce-scatter.4
  104.9 29.7 all-gather.2
  140.2 65.0 all-reduce.2
  212.6 41.4 reduce-scatter.8
  257.0 41.7 reduce-scatter.10
  301.2 29.7 all-gather.4
  336.6 65.0 all-reduce.4
where the time goes:
time: 412 us; the launch traced here: 411 us
  waiting for transfers between devices  332 us (81%)
  matrix products  31.6 us (8%)
  blocking collectives  22.2 us (5%)
  between operations  13.5 us (3%)
  other arithmetic  9.81 us (2%)
    psum x2, waiting for transfers between devices, body(): branch = lax.psum(partial_down, 'cb')  130 us
    reduce_scatter x2, waiting for transfers between devices, body(): lax.psum_scatter(up_part, 'ra', scatter_dimension=1, tiled=True)  70.9 us
    reduce_scatter x2, waiting for transfers between devices, body(): lax.psum_scatter(gate_part, 'ra', scatter_dimension=1, tiled=True)  70.8 us
    all_gather x2, waiting for transfers between devices, body(): hidden = lax.all_gather(share, 'ra', axis=1, tiled=True)  59.7 us
    psum x2, blocking collectives, body(): total = lax.psum(squares, 'ra')  22.2 us
    dot_general x2, matrix products, body(): jnp.dot(hidden, down_weight[layer], preferred_element_type=jnp.float32)  10.8 us
    dot_general x2, matrix products, body(): jnp.dot(normed, up_weight[layer], preferred_element_type=jnp.float32)  10.6 us
    dot_general x2, matrix products, body(): jnp.dot(normed, gate_weight[layer], preferred_element_type=jnp.float32)  10.2 us
  transfers between devices with their start and end apart: 8, of which 8 were waited for; matrix products, arithmetic and copies ran while one was open for 3% of the time, Pallas kernels for 0%

commit v1 on v0

--- a/solution.py
+++ b/solution.py
@@ -26,7 +26,9 @@
         share = (jax.nn.silu(gate_share * scale) * (up_share * scale)).astype(jnp.bfloat16)
         hidden = lax.all_gather(share, "ra", axis=1, tiled=True)
         partial_down = jnp.dot(hidden, down_weight[layer], preferred_element_type=jnp.float32)
-        branch = lax.psum(partial_down, "cb")
+        branch = partial_down
+        for hop in (1, 2, 4):
+            branch = branch + lax.ppermute(branch, "cb", [(dev, dev ^ hop) for dev in range(8)])
         stream = (keep_share * widened + branch).astype(jnp.bfloat16)
     return stream
 

time: 412 us -> 566 us (1.37)
  waiting for transfers between devices: 332 us -> 484 us
  starting transfers between devices: 0.3 us -> 8.4 us
    ppermute x0 -> x6, waiting for transfers between devices: none -> 281 us  [body(): lax.ppermute(branch, 'cb', [(dev, dev ^ hop) for dev in range(8)])]
    psum x2 -> x0, waiting for transfers between devices: 130 us -> none  [body(): branch = lax.psum(partial_down, 'cb')]
    ppermute x0 -> x6, starting transfers between devices: none -> 8.19 us  [body(): lax.ppermute(branch, 'cb', [(dev, dev ^ hop) for dev in range(8)])]
  transfers between devices with their start and end apart: 8 -> 12, of which waited for: 8 -> 12; matrix products, arithmetic and copies ran while one was open for 3% -> 2% of each run, Pallas kernels for 0% -> 0%
where the time goes in v1:
time: 566 us; the launch traced here: 565 us
  waiting for transfers between devices  484 us (86%)
  matrix products  27.1 us (5%)
  blocking collectives  21.5 us (4%)
  between operations  13.6 us (2%)
  other arithmetic  8.98 us (2%)
  starting transfers between devices  8.4 us (1%)
    ppermute x6, waiting for transfers between devices, body(): lax.ppermute(branch, 'cb', [(dev, dev ^ hop) for dev in range(8)])  281 us
    reduce_scatter x2, waiting for transfers between devices, body(): lax.psum_scatter(gate_part, 'ra', scatter_dimension=1, tiled=True)  72 us
    reduce_scatter x2, waiting for transfers between devices, body(): lax.psum_scatter(up_part, 'ra', scatter_dimension=1, tiled=True)  70.9 us
    all_gather x2, waiting for transfers between devices, body(): hidden = lax.all_gather(share, 'ra', axis=1, tiled=True)  59.7 us
    psum x2, blocking collectives, body(): total = lax.psum(squares, 'ra')  21.5 us
  transfers between devices with their start and end apart: 12, of which 12 were waited for; matrix products, arithmetic and copies ran while one was open for 2% of the time, Pallas kernels for 0%

profile of v1, /device:TPU:0, one launch (start us, length us, event | category | flops | bytes accessed | tf_op | source)
XLA Modules:
  0.0 565.5 jit_solution(5909414072514984765)
XLA Ops:
  6.5 0.8 fusion.31
  7.3 5.4 fusion.8
  12.8 1.1 copy-done
  14.0 5.1 fusion.10
  19.4 11.9 %psum.14 = f32[512]{0:T(512)S(1)} all-reduce(f32[512]{0:T(512)S(1)} %fusion.21), channel_id=1, replica_groups=mesh['ra'=4,'cb'=8] {'ra'}, use_global_device_ids=true, to_apply=%region_2.0 | all-reduce | flops 512 | bytes 4096 | tf_op jit(solution)/shard_map/psum | solution.py:20
  31.3 26.3 %reduce-scatter.7.cloned.1.call-done = f32[512,352]{0,1:T(8,128)} async-done(((f32[512,1408]{0,1:T(8,128)}), f32[512,352]{0,1:T(8,128)}) %reduce-scatter.7.cloned.1.call-update) | async-done | bytes 720912 | tf_op jit(solution)/shard_map/reduce_scatter | solution.py:23
  57.6 44.8 %reduce-scatter.5.cloned.1.call-done = f32[512,352]{0,1:T(8,128)} async-done(((f32[512,1408]{0,1:T(8,128)}), f32[512,352]{0,1:T(8,128)}) %reduce-scatter.5.cloned.1.call-update) | async-done | bytes 720912 | tf_op jit(solution)/shard_map/reduce_scatter | solution.py:22
  102.4 2.3 multiply_convert_fusion.1
  104.8 29.8 %all-gather.3.cloned.1.call-done = bf16[512,1408]{0,1:T(8,128)(2,1)} async-done(((bf16[512,352]{0,1:T(8,128)(2,1)}), bf16[512,1408]{0,1:T(8,128)(2,1)}) %all-gather.3.cloned.1.call-update) | async-done | bytes 1441808 | tf_op jit(solution)/shard_map/all_gather | solution.py:27
  134.6 4.1 fusion.6
  138.8 4.1 collective-permute-done
  142.9 0.6 add.51
  143.5 1.6 collective-permute-start.1
  145.0 46.2 %collective-permute-done.1 = f32[512,1024]{1,0:T(8,128)S(1)} collective-permute-done((f32[512,1024]{1,0:T(8,128)S(1)}, f32[512,1024]{1,0:T(8,128)S(1)}, u32[]{:S(2)}, u32[]{:S(2)}) %collective-permute-start.1) | collective-permute-done | bytes 2097184 | tf_op jit(solution)/shard_map/ppermute | solution.py:31
  191.7 2.5 collective-permute-start.2
  194.1 90.2 %collective-permute-done.2 = f32[512,1024]{1,0:T(8,128)S(1)} collective-permute-done((f32[512,1024]{1,0:T(8,128)S(1)}, f32[512,1024]{1,0:T(8,128)S(1)}, u32[]{:S(2)}, u32[]{:S(2)}) %collective-permute-start.2) | collective-permute-done | bytes 2097184 | tf_op jit(solution)/shard_map/ppermute | solution.py:31
  284.4 0.6 fusion.25
  285.0 3.3 fusion.4
  288.3 5.1 fusion.2
  293.5 9.6 %psum.15 = f32[512]{0:T(512)S(1)} all-reduce(f32[512]{0:T(512)S(1)} %get-tuple-element.5), channel_id=1, replica_groups=mesh['ra'=4,'cb'=8] {'ra'}, use_global_device_ids=true, to_apply=%region_6.7 | all-reduce | flops 512 | bytes 4096 | tf_op jit(solution)/shard_map/psum | solution.py:20
  303.2 27.2 %reduce-scatter.9.cloned.1.call-done = f32[512,352]{0,1:T(8,128)} async-done(((f32[512,1408]{0,1:T(8,128)}), f32[512,352]{0,1:T(8,128)}) %reduce-scatter.9.cloned.1.call-update) | async-done | bytes 720912 | tf_op jit(solution)/shard_map/reduce_scatter | solution.py:22
  330.4 44.7 %reduce-scatter.11.cloned.1.call-done = f32[512,352]{0,1:T(8,128)} async-done(((f32[512,1408]{0,1:T(8,128)}), f32[512,352]{0,1:T(8,128)}) %reduce-scatter.11.cloned.1.call-update) | async-done | bytes 720912 | tf_op jit(solution)/shard_map/reduce_scatter | solution.py:23
  375.0 2.3 multiply_convert_fusion
  377.3 29.9 %all-gather.5.cloned.1.call-done = bf16[512,1408]{0,1:T(8,128)(2,1)} async-done(((bf16[512,352]{0,1:T(8,128)(2,1)}), bf16[512,1408]{0,1:T(8,128)(2,1)}) %all-gather.5.cloned.1.call-update) | async-done | bytes 1441808 | tf_op jit(solution)/shard_map/all_gather | solution.py:27
  407.2 4.1 fusion
  411.4 4.1 collective-permute-done.3
  415.5 0.6 add.57
  416.1 1.6 collective-permute-start.4
  417.6 46.2 %collective-permute-done.4 = f32[512,1024]{1,0:T(8,128)S(1)} collective-permute-done((f32[512,1024]{1,0:T(8,128)S(1)}, f32[512,1024]{1,0:T(8,128)S(1)}, u32[]{:S(2)}, u32[]{:S(2)}) %collective-permute-start.4) | collective-permute-done | bytes 2097184 | tf_op jit(solution)/shard_map/ppermute | solution.py:31
  464.3 2.5 collective-permute-start.5
  466.7 90.2 %collective-permute-done.5 = f32[512,1024]{1,0:T(8,128)S(1)} collective-permute-done((f32[512,1024]{1,0:T(8,128)S(1)}, f32[512,1024]{1,0:T(8,128)S(1)}, u32[]{:S(2)}, u32[]{:S(2)}) %collective-permute-start.5) | collective-permute-done | bytes 2097184 | tf_op jit(solution)/shard_map/ppermute | solution.py:31
  557.0 1.6 fusion.23
  (25 shorter events, 1.6 us)
Async XLA Ops:
  6.5 51.1 %reduce-scatter.7.cloned.1.call-start = ((), (), s32[]{:S(2)}) async-start(), calls=%async_computation.5 | async-start | bytes 3604480 | tf_op jit(solution)/shard_map/reduce_scatter | solution.py:23
  12.7 1.2 copy-start
  12.8 89.7 %reduce-scatter.5.cloned.1.call-start = ((), (), s32[]{:S(2)}) async-start(), calls=%async_computation.4 | async-start | bytes 3604480 | tf_op jit(solution)/shard_map/reduce_scatter | solution.py:22
  19.1 115.5 %all-gather.3.cloned.1.call-start = ((), (), s32[]{:S(2)}) async-start(), calls=%async_computation.6 | async-start | bytes 1802240 | tf_op jit(solution)/shard_map/all_gather | solution.py:27
  104.7 225.6 %reduce-scatter.9.cloned.1.call-start = ((), (), s32[]{:S(2)}) async-start(), calls=%async_computation.7 | async-start | bytes 3604480 | tf_op jit(solution)/shard_map/reduce_scatter | solution.py:22
  138.7 4.2 collective-permute-start
  142.9 142.0 %slice-start = ((s8[5767168]{0:T(1024)(128)(4,1)}), s8[4194304]{0:T(1024)(128)(4,1)S(1)}, s32[]{:S(2)}) async-start(s8[5767168]{0:T(1024)(128)(4,1)} %bitcast.26), calls=%async_computation.10 | async-start | bytes 8388608
  143.5 141.5 %slice-start.1 = ((s8[5767168]{0:T(1024)(128)(4,1)}), s8[1572864]{0:T(1024)(128)(4,1)S(1)}, s32[]{:S(2)}) async-start(s8[5767168]{0:T(1024)(128)(4,1)} %bitcast.26), calls=%async_computation.11 | async-start | bytes 3145728
  143.5 47.7 %collective-permute-start.1 = (f32[512,1024]{1,0:T(8,128)S(1)}, f32[512,1024]{1,0:T(8,128)S(1)}, u32[]{:S(2)}, u32[]{:S(2)}) collective-permute-start(f32[512,1024]{1,0:T(8,128)S(1)} %add.51), channel_id=1, source_target_pairs={{0,2},{1,3},{2,0},{3,1},{4,6},{5,7},{6,4},{7,5},{8,10},{9,11},{10,... | collective-permute-start | bytes 6291464 | tf_op jit(solution)/shard_map/ppermute | solution.py:31
  191.7 92.7 %collective-permute-start.2 = (f32[512,1024]{1,0:T(8,128)S(1)}, f32[512,1024]{1,0:T(8,128)S(1)}, u32[]{:S(2)}, u32[]{:S(2)}) collective-permute-start(f32[512,1024]{1,0:T(8,128)S(1)} %add.52), channel_id=1, source_target_pairs={{0,4},{1,5},{2,6},{3,7},{4,0},{5,1},{6,2},{7,3},{8,12},{9,13},{10,... | collective-permute-start | bytes 6291464 | tf_op jit(solution)/shard_map/ppermute | solution.py:31
  288.3 86.8 %reduce-scatter.11.cloned.1.call-start = ((), (), s32[]{:S(2)}) async-start(), calls=%async_computation.8 | async-start | bytes 3604480 | tf_op jit(solution)/shard_map/reduce_scatter | solution.py:23
  293.5 113.8 %all-gather.5.cloned.1.call-start = ((), (), s32[]{:S(2)}) async-start(), calls=%async_computation.9 | async-start | bytes 1802240 | tf_op jit(solution)/shard_map/all_gather | solution.py:27
  411.3 4.2 collective-permute-start.3
  416.1 47.7 %collective-permute-start.4 = (f32[512,1024]{1,0:T(8,128)S(1)}, f32[512,1024]{1,0:T(8,128)S(1)}, u32[]{:S(2)}, u32[]{:S(2)}) collective-permute-start(f32[512,1024]{1,0:T(8,128)S(1)} %add.57), channel_id=1, source_target_pairs={{0,2},{1,3},{2,0},{3,1},{4,6},{5,7},{6,4},{7,5},{8,10},{9,11},{10,... | collective-permute-start | bytes 6291464 | tf_op jit(solution)/shard_map/ppermute | solution.py:31
  464.3 92.7 %collective-permute-start.5 = (f32[512,1024]{1,0:T(8,128)S(1)}, f32[512,1024]{1,0:T(8,128)S(1)}, u32[]{:S(2)}, u32[]{:S(2)}) collective-permute-start(f32[512,1024]{1,0:T(8,128)S(1)} %add.58), channel_id=1, source_target_pairs={{0,4},{1,5},{2,6},{3,7},{4,0},{5,1},{6,2},{7,3},{8,12},{9,13},{10,... | collective-permute-start | bytes 6291464 | tf_op jit(solution)/shard_map/ppermute | solution.py:31
Sparse Core Ops, SparseCore 0:
  12.9 44.7 reduce-scatter.6
  60.7 41.7 reduce-scatter.4
  104.9 29.7 all-gather.2
  288.4 41.9 reduce-scatter.8
  333.3 41.7 reduce-scatter.10
  377.5 29.7 all-gather.4
